TPU v7x, 512 devices: a whole 4x8x8 slice. The times are simulated.
512 devices in a mesh: rep: 2 (over z_hi), fs: 32 (over z_lo, y), tp: 8 (over x, core).
Axes of the slice: x: 4, y: 8, z: 8 (z_hi: 2, z_lo: 4; z = z_hi * 4 + z_lo), core: 2. Of those that a mesh axis runs over, the one named last changes fastest.
Arguments:
- tokens: bfloat16 [32768, 2048], P(('rep', 'fs'), 'tp'), may hold values from -6 to 6
- mix_gain: float32 [2048], replicated, may hold values from 0.1 to 1.9
- query_w: bfloat16 [2048, 2048], P('fs', 'tp'), may hold values from -0.125 to 0.125
- key_w: bfloat16 [2048, 2048], P('fs', 'tp'), may hold values from -0.125 to 0.125
- value_w: bfloat16 [2048, 4096], P('fs', 'tp'), may hold values from -0.125 to 0.125
- head_gain: float32 [8, 512], replicated, may hold values from 0.1 to 1.9
- out_w: bfloat16 [4096, 2048], P('tp', 'fs'), may hold values from -0.09375 to 0.09375
- chan_gain: float32 [2048], replicated, may hold values from 0.1 to 1.9
- up_w: bfloat16 [2048, 4096], P('fs', 'tp'), may hold values from -0.125 to 0.125
- down_w: bfloat16 [4096, 2048], P('tp', 'fs'), may hold values from -0.09375 to 0.09375
Outputs:
- layer_out: bfloat16 [32768, 2048], P(('rep', 'fs'), 'tp')
All inputs are finite; a program needn't handle non-finite values.
Results may differ from a plain program's by a relative error of at most 0.019.
Values may be sent and summed in bfloat16 or wider, within the bound.
A program may use at most 64 MiB of HBM per device.

v0:
```python
import jax
import jax.numpy as jnp
from jax import lax
from jax.sharding import PartitionSpec as P

DK = 256
DV = 512
BLOCK = 128
EPS = 1e-06
HEAD_EPS = 0.05
THETA = 10000.0


def gather_turned(arrays, axis, dims):
    turned = [jnp.moveaxis(a, dim, 0) for a, dim in zip(arrays, dims)]
    both = jnp.concatenate([t.reshape(len(t), -1) for t in turned], axis=1)
    whole, at, finished = (lax.all_gather(both, axis, axis=0, tiled=True), 0, [])
    for t, dim in zip(turned, dims):
        section = whole[:, at : at + t[0].size].reshape(-1, *t.shape[1:])
        finished.append(jnp.moveaxis(section, 0, dim))
        at += t[0].size
    return tuple(finished)


def in_order(blocks, dim):
    shape = list(blocks.shape[1:])
    shape[dim] *= blocks.shape[0]
    return jnp.moveaxis(blocks, 0, dim).reshape(shape)


def copy_for_each(value, axis):
    count = lax.axis_size(axis)
    return lax.all_to_all(
        jnp.broadcast_to(value[None], (count, *value.shape)), axis, 0, 0, tiled=True
    )


def gathered_copies(value, axis, dim):
    return in_order(copy_for_each(value, axis), dim)


def cut_along(value, dim, count):
    shape = value.shape
    blocks = value.reshape(*shape[:dim], count, shape[dim] // count, *shape[dim + 1 :])
    return jnp.moveaxis(blocks, dim, 0)


def sum_at_owner(value, axis, dim):
    count = lax.axis_size(axis)
    blocks = lax.all_to_all(cut_along(value, dim, count), axis, 0, 0, tiled=True)
    return jnp.sum(blocks.astype(jnp.float32), axis=0)


def norm_rows(rows, gain):
    values = rows.astype(jnp.float32)
    scale = lax.rsqrt(jnp.mean(values * values, axis=-1, keepdims=True) + EPS)
    return (values * scale * gain).astype(jnp.bfloat16)


def rotate(field, places):
    half = field.shape[-1] // 2
    inverse = THETA ** (-jnp.arange(half, dtype=jnp.float32) / half)
    angles = places[:, None] * inverse
    cosine = jnp.cos(angles)[:, None, :]
    sine = jnp.sin(angles)[:, None, :]
    first = field[..., :half]
    second = field[..., half:]
    return jnp.concatenate(
        [first * cosine - second * sine, second * cosine + first * sine], axis=-1
    )


def retain(query, keys, values, log_rate):
    count = query.shape[0] // BLOCK
    q_blocks = query.reshape(count, BLOCK, query.shape[1])
    k_blocks = keys.reshape(count, BLOCK, keys.shape[1])
    v_blocks = values.reshape(count, BLOCK, values.shape[1])
    place = jnp.arange(BLOCK, dtype=jnp.float32)
    offset = place[:, None] - place[None, :]
    mask = jnp.where(offset >= 0, jnp.exp(log_rate * jnp.maximum(offset, 0.0)), 0.0)
    q_decay = jnp.exp(log_rate * (place + 1.0))
    k_decay = jnp.exp(log_rate * (BLOCK - 1.0 - place))
    block_decay = jnp.exp(log_rate * BLOCK)

    def advance(state, item):
        q_part, k_part, v_part = item
        scores = jnp.dot(q_part, k_part.T, preferred_element_type=jnp.float32)
        weights = (scores * mask).astype(jnp.bfloat16)
        result = jnp.dot(weights, v_part, preferred_element_type=jnp.float32)
        q_scaled = (q_part.astype(jnp.float32) * q_decay[:, None]).astype(jnp.bfloat16)
        result = result + jnp.dot(
            q_scaled, state.astype(jnp.bfloat16), preferred_element_type=jnp.float32
        )
        k_scaled = (k_part.astype(jnp.float32) * k_decay[:, None]).astype(jnp.bfloat16)
        state = state * block_decay + jnp.dot(
            k_scaled.T, v_part, preferred_element_type=jnp.float32
        )
        return (state, result)

    start = jnp.zeros((query.shape[1], values.shape[1]), jnp.float32)
    _, outputs = lax.scan(advance, start, (q_blocks, k_blocks, v_blocks))
    return outputs.reshape(count * BLOCK, values.shape[1])


def shards(tokens, mix_gain, query_w, key_w, value_w, head_gain, out_w, chan_gain, up_w, down_w):
    rows = tokens.shape[0]
    local = query_w.shape[1] // DK
    query_all, key_all, value_all, out_all, up_all, down_all = gather_turned(
        (query_w, key_w, value_w, out_w, up_w, down_w), "fs", (0, 0, 0, 1, 0, 1)
    )
    whole = gathered_copies(tokens, "tp", 1)
    normed = norm_rows(whole, mix_gain)
    qraw = jnp.dot(normed, query_all, preferred_element_type=jnp.float32)
    kraw = jnp.dot(normed, key_all, preferred_element_type=jnp.float32)
    vraw = jnp.dot(normed, value_all, preferred_element_type=jnp.float32)
    places = jnp.arange(rows, dtype=jnp.int32).astype(jnp.float32)
    query = rotate(qraw.reshape(rows, local, DK), places).astype(jnp.bfloat16)
    keys = (rotate(kraw.reshape(rows, local, DK), places) * DK ** (-0.5)).astype(jnp.bfloat16)
    values = vraw.reshape(rows, local, DV).astype(jnp.bfloat16)
    first_head = lax.axis_index("tp") * local
    heads = (first_head + jnp.arange(local, dtype=jnp.int32)).astype(jnp.float32)
    log_rate = jnp.log1p(-jnp.exp2(-5.0 - heads))
    retained = jax.vmap(retain, in_axes=(1, 1, 1, 0), out_axes=1)(query, keys, values, log_rate)
    gains = lax.dynamic_slice_in_dim(head_gain, first_head, local, 0)
    scale = lax.rsqrt(jnp.mean(retained * retained, axis=-1, keepdims=True) + HEAD_EPS)
    head_out = (retained * scale * gains).astype(jnp.bfloat16).reshape(rows, local * DV)
    mixer_terms = jnp.dot(head_out, out_all, preferred_element_type=jnp.float32)
    mixed = sum_at_owner(mixer_terms.astype(jnp.bfloat16), "tp", 1)
    middle = (tokens.astype(jnp.float32) + mixed).astype(jnp.bfloat16)
    whole_middle = gathered_copies(middle, "tp", 1)
    chan_normed = norm_rows(whole_middle, chan_gain)
    upward = jnp.dot(chan_normed, up_all, preferred_element_type=jnp.float32)
    hidden = jnp.square(jax.nn.relu(upward)).astype(jnp.bfloat16)
    chan_terms = jnp.dot(hidden, down_all, preferred_element_type=jnp.float32)
    channel = sum_at_owner(chan_terms.astype(jnp.bfloat16), "tp", 1)
    return (middle.astype(jnp.float32) + channel).astype(jnp.bfloat16)


def solution(mesh):
    placed = (
        P(("rep", "fs"), "tp"),
        P(),
        P("fs", "tp"),
        P("fs", "tp"),
        P("fs", "tp"),
        P(),
        P("tp", "fs"),
        P(),
        P("fs", "tp"),
        P("tp", "fs"),
    )
    return jax.shard_map(
        shards, mesh=mesh, in_specs=placed, out_specs=P(("rep", "fs"), "tp"), check_vma=False
    )
```

profile of v0, /device:TPU:1, one launch (start us, length us, event | category | flops | bytes accessed | tf_op | source)
XLA Modules:
  0.0 313.0 jit_solution(4496840921103430434)
XLA Ops:
  6.5 0.8 constant_dynamic-update-slice_fusion.3
  7.3 0.8 constant_dynamic-update-slice_fusion.2
  8.1 0.8 constant_dynamic-update-slice_fusion.1
  8.9 0.8 bitcast_dynamic-update-slice_fusion.1
  9.8 0.8 constant_dynamic-update-slice_fusion
  10.6 0.8 bitcast_dynamic-update-slice_fusion
  12.2 1.1 copy.23
  13.3 1.5 broadcast_in_dim.15
  14.8 10.3 %all-to-all-start = ((bf16[8,512,256]{1,2,0:T(8,128)(2,1)}), bf16[8,512,256]{1,2,0:T(8,128)(2,1)S(1)}, u32[]{:S(2)}, u32[]{:S(2)}) async-start(bf16[8,512,256]{1,2,0:T(8,128)(2,1)} %broadcast_in_dim.15), calls=%async_computation | async-start | bytes 4194304 | tf_op jit(solution)/shard_map/all_to_all | solution.py:33
  25.3 26.1 %all-to-all-done = bf16[8,512,256]{1,2,0:T(8,128)(2,1)S(1)} async-done(((bf16[8,512,256]{1,2,0:T(8,128)(2,1)}), bf16[8,512,256]{1,2,0:T(8,128)(2,1)S(1)}, u32[]{:S(2)}, u32[]{:S(2)}) %all-to-all-start) | async-done | bytes 2097184 | tf_op jit(solution)/shard_map/all_to_all | solution.py:33
  52.0 1.9 fusion.57
  53.8 117.0 %all-gather.2.cloned.1.call-done = bf16[2048,2560]{1,0:T(8,128)(2,1)} async-done(((bf16[64,2560]{1,0:T(8,128)(2,1)}), bf16[2048,2560]{1,0:T(8,128)(2,1)}) %all-gather.2.cloned.1.call-update) | async-done | bytes 10485776 | tf_op jit(solution)/shard_map/all_gather | solution.py:17
  170.9 2.6 convolution_bitcast_fusion.2
  173.5 2.0 convolution_bitcast_fusion.1
  175.5 1.2 fusion.95
  177.0 3.0 fusion.70
  180.0 3.8 %while.15 = (s32[]{:T(128)}, f32[1,256,512]{2,1,0:T(8,128)S(1)}, f32[4,1,128,512]{3,2,1,0:T(8,128)S(1)}, f32[1]{0:T(128)}, bf16[4,1,128,256]{3,2,1,0:T(8,128)(2,...) while((s32[]{:T(128)}, f32[1,256,512]{2,1,0:T(8,128)S(1)}, ...), condition=%wide.region_2.3_spmd.clone.clone.clone, body=%wide.region_1.2_spmd.clone.clone.clone.sunk | while | flops 93176320 | bytes 2890356 | solution.py:101
  184.2 2.9 convolution_convert_fusion.1
  187.2 49.3 %all_to_all.20 = bf16[8,512,256]{2,1,0:T(8,128)(2,1)S(1)} all-to-all(bf16[8,512,256]{2,1,0:T(8,128)(2,1)S(1)} %bitcast.148), channel_id=1, replica_groups=mesh['rep'=2,'fs'=32,'tp'=8] {'tp'}, dimensions={0} | all-to-all | bytes 4194304 | tf_op jit(solution)/shard_map/all_to_all | solution.py:50
  237.8 29.7 %all_to_all.21 = bf16[8,512,256]{1,2,0:T(8,128)(2,1)S(1)} all-to-all(bf16[8,512,256]{1,2,0:T(8,128)(2,1)S(1)} %broadcast_in_dim.16), channel_id=1, replica_groups=mesh['rep'=2,'fs'=32,'tp'=8] {'tp'}, dimensions={0} | all-to-all | bytes 4194304 | tf_op jit(solution)/shard_map/all_to_all | solution.py:33
  268.2 1.9 fusion.55
  270.0 5.2 %convolution_convert_fusion = bf16[512,2048]{1,0:T(8,128)(2,1)S(1)} fusion(bf16[2048,2560]{1,0:T(8,128)(2,1)} %all-gather.2.cloned.1.call-done, bf16[512,2048]{0,1:T(8,128)(2,1)} %fusion.55), kind=kOutput, calls=%fused_computation.61 | convolution fusion | flops 2149318656 | bytes 8388608 | tf_op jit(solution)/shard_map/dot_general | solution.py:134
  275.4 29.7 %all_to_all.22 = bf16[8,512,256]{2,1,0:T(8,128)(2,1)S(1)} all-to-all(bf16[8,512,256]{2,1,0:T(8,128)(2,1)S(1)} %bitcast.149), channel_id=1, replica_groups=mesh['rep'=2,'fs'=32,'tp'=8] {'tp'}, dimensions={0} | all-to-all | bytes 4194304 | tf_op jit(solution)/shard_map/all_to_all | solution.py:50
  305.4 0.8 add_convert_fusion
  (55 shorter events, 8.1 us)
Async XLA Ops:
  6.5 18.7 %copy-start = (f32[8,512]{1,0:T(8,128)S(1)}, f32[8,512]{1,0:T(8,128)}, u32[]{:S(2)}) copy-start(f32[8,512]{1,0:T(8,128)} %param.17) | copy-start | bytes 49156
  6.5 164.3 %all-gather.2.cloned.1.call-start = ((), (), s32[]{:S(2)}) async-start(), calls=%async_computation.4 | async-start | bytes 10813440 | tf_op jit(solution)/shard_map/all_gather | solution.py:17
  11.4 0.7 copy-start.5
  14.8 36.7 %all-to-all-start = ((bf16[8,512,256]{1,2,0:T(8,128)(2,1)}), bf16[8,512,256]{1,2,0:T(8,128)(2,1)S(1)}, u32[]{:S(2)}, u32[]{:S(2)}) async-start(bf16[8,512,256]{1,2,0:T(8,128)(2,1)} %broadcast_in_dim.15), calls=%async_computation | async-start | bytes 4194304 | tf_op jit(solution)/shard_map/all_to_all | solution.py:33
  25.1 26.9 %copy-start.6 = (f32[2048]{0:T(1024)S(1)}, f32[2048]{0:T(1024)}, u32[]{:S(2)}) copy-start(f32[2048]{0:T(1024)} %param.13) | copy-start | bytes 24580
  53.8 119.6 %copy-start.2 = (bf16[512,2048]{0,1:T(8,128)(2,1)S(1)}, bf16[512,2048]{0,1:T(8,128)(2,1)}, u32[]{:S(2)}) copy-start(bf16[512,2048]{0,1:T(8,128)(2,1)} %fusion.57) | copy-start | bytes 6291460
  175.5 1.6 copy-start.3
  177.0 3.0 copy-start.1
  236.5 1.0 copy-start.4
  267.5 0.7 copy-start.7
Sparse Core Ops, SparseCore 0:
  12.3 158.5 all-gather.1
where the time goes:
time: 314 us; the launch traced here: 313 us
  waiting for transfers between devices  143 us (46%)
  blocking collectives  109 us (35%)
  matrix products  19.2 us (6%)
  between operations  13.7 us (4%)
  starting transfers between devices  10.3 us (3%)
  local copies, waits for them, and re-layouts  9.88 us (3%)
  other arithmetic  7.86 us (3%)
    all_gather x1, waiting for transfers between devices, gather_turned(): lax.all_gather(both, axis, axis=0, tiled=True)  117 us
    all_to_all x2, blocking collectives, sum_at_owner(): lax.all_to_all(cut_along(value, dim, count), axis, 0, 0, tiled=True)  78.9 us
    all_to_all x1, blocking collectives, copy_for_each(): lax.all_to_all(jnp.broadcast_to(value[None], (count, *value.shape)), axis...  29.7 us
    all_to_all x1, waiting for transfers between devices, copy_for_each(): lax.all_to_all(jnp.broadcast_to(value[None], (count, *value.shape)), axis...  26.1 us
    all_to_all x1, starting transfers between devices, copy_for_each(): lax.all_to_all(jnp.broadcast_to(value[None], (count, *value.shape)), axis...  10.3 us
    unnamed x22, local copies, waits for them, and re-layouts  6.96 us
  transfers between devices with their start and end apart: 2, of which 2 were waited for; matrix products, arithmetic and copies ran while one was open for 2% of the time, Pallas kernels for 0%

commit v1 on v0

--- a/solution.py
+++ b/solution.py
@@ -14,7 +14,14 @@
 def gather_turned(arrays, axis, dims):
     turned = [jnp.moveaxis(a, dim, 0) for a, dim in zip(arrays, dims)]
     both = jnp.concatenate([t.reshape(len(t), -1) for t in turned], axis=1)
-    whole, at, finished = (lax.all_gather(both, axis, axis=0, tiled=True), 0, [])
+
+    def pack_roads(piece_in):
+        all_values = tuple((piece_in for _ in range(lax.axis_size(axis))))
+        o_now = jnp.stack(all_values)
+        state_next = lax.all_to_all(o_now, axis, 0, 0)
+        return jnp.concatenate(state_next, axis=0)
+
+    whole, at, finished = (pack_roads(both), 0, [])
     for t, dim in zip(turned, dims):
         section = whole[:, at : at + t[0].size].reshape(-1, *t.shape[1:])
         finished.append(jnp.moveaxis(section, 0, dim))

time: 314 us -> 484 us (1.54)
  the two profiles are of different devices: /device:TPU:1 before, /device:TPU:120 now
where the time goes in v1:
time: 484 us; the launch traced here: 483 us
  waiting for transfers between devices  341 us (70%)
  blocking collectives  89 us (18%)
  matrix products  19.2 us (4%)
  starting transfers between devices  16 us (3%)
  local copies, waits for them, and re-layouts  9.12 us (2%)
  other arithmetic  7.88 us (2%)
    all_to_all x1, waiting for transfers between devices, pack_roads(): state_next = lax.all_to_all(o_now, axis, 0, 0)  314 us
    all_to_all x2, blocking collectives, sum_at_owner(): lax.all_to_all(cut_along(value, dim, count), axis, 0, 0, tiled=True)  59.3 us
    all_to_all x1, blocking collectives, copy_for_each(): lax.all_to_all(jnp.broadcast_to(value[None], (count, *value.shape)), axis...  29.7 us
    all_to_all x1, waiting for transfers between devices, copy_for_each(): lax.all_to_all(jnp.broadcast_to(value[None], (count, *value.shape)), axis...  27 us
    all_to_all x1, starting transfers between devices, pack_roads(): state_next = lax.all_to_all(o_now, axis, 0, 0)  11.6 us
  transfers between devices with their start and end apart: 2, of which 2 were waited for; matrix products, arithmetic and copies ran while one was open for 1% of the time, Pallas kernels for 0%

profile of v1, /device:TPU:120, one launch (start us, length us, event | category | flops | bytes accessed | tf_op | source)
XLA Modules:
  0.0 483.1 jit_solution(8598965904112530689)
XLA Ops:
  0.0 1.1 copy.23
  1.1 1.5 broadcast_in_dim.15
  2.7 4.4 all-to-all-start
  7.2 27.0 %all-to-all-done = bf16[8,512,256]{1,2,0:T(8,128)(2,1)S(1)} async-done(((bf16[8,512,256]{1,2,0:T(8,128)(2,1)}), bf16[8,512,256]{1,2,0:T(8,128)(2,1)S(1)}, u32[]{:S(2)}, u32[]{:S(2)}) %all-to-all-start) | async-done | bytes 2097184 | tf_op jit(solution)/shard_map/all_to_all | solution.py:40
  34.3 5.0 %stack.2 = bf16[32,64,2560]{2,1,0:T(8,128)(2,1)} broadcast(bf16[64,2560]{1,0:T(8,128)(2,1)S(1)} %bitcast_dynamic-update-slice_fusion), dimensions={1,2} | broadcast | bytes 10813440 | tf_op jit(solution)/shard_map/stack | solution.py:20
  39.3 11.6 %all-to-all-start.1 = ((bf16[32,64,2560]{2,1,0:T(8,128)(2,1)}), bf16[32,64,2560]{2,1,0:T(8,128)(2,1)}, u32[]{:S(2)}, u32[]{:S(2)}) async-start(bf16[32,64,2560]{2,1,0:T(8,128)(2,1)} %stack.2), calls=%async_computation.1 | async-start | bytes 20971520 | tf_op jit(solution)/shard_map/all_to_all | solution.py:21
  51.1 0.5 multiply_reduce_fusion.1
  51.6 1.9 fusion.57
  53.5 314.2 %all-to-all-done.1 = bf16[32,64,2560]{2,1,0:T(8,128)(2,1)} async-done(((bf16[32,64,2560]{2,1,0:T(8,128)(2,1)}), bf16[32,64,2560]{2,1,0:T(8,128)(2,1)}, u32[]{:S(2)}, u32[]{:S(2)}) %all-to-all-start.1) | async-done | bytes 10485792 | tf_op jit(solution)/shard_map/all_to_all | solution.py:21
  367.7 2.7 convolution_bitcast_fusion.2
  370.5 2.0 convolution_bitcast_fusion.1
  372.4 2.9 fusion.70
  375.3 1.2 fusion.95
  376.7 3.8 while.15
  376.7 0.3 fusion.122
  380.8 2.9 convolution_convert_fusion.1
  383.8 29.7 %all_to_all.25 = bf16[8,512,256]{2,1,0:T(8,128)(2,1)S(1)} all-to-all(bf16[8,512,256]{2,1,0:T(8,128)(2,1)S(1)} %bitcast.149), channel_id=1, replica_groups=mesh['rep'=2,'fs'=32,'tp'=8] {'tp'}, dimensions={0} | all-to-all | bytes 4194304 | tf_op jit(solution)/shard_map/all_to_all | solution.py:57
  413.8 0.6 copy-done.3
  414.8 29.7 %all_to_all.26 = bf16[8,512,256]{1,2,0:T(8,128)(2,1)S(1)} all-to-all(bf16[8,512,256]{1,2,0:T(8,128)(2,1)S(1)} %broadcast_in_dim.16), channel_id=1, replica_groups=mesh['rep'=2,'fs'=32,'tp'=8] {'tp'}, dimensions={0} | all-to-all | bytes 4194304 | tf_op jit(solution)/shard_map/all_to_all | solution.py:40
  444.5 0.5 multiply_reduce_fusion
  445.2 1.9 fusion.55
  447.0 5.2 %convolution_convert_fusion = bf16[512,2048]{1,0:T(8,128)(2,1)S(1)} fusion(bf16[2048,2560]{1,0:T(8,128)(2,1)} %bitcast.5, bf16[512,2048]{0,1:T(8,128)(2,1)} %fusion.55), kind=kOutput, calls=%fused_computation.61 | convolution fusion | flops 2149318656 | bytes 8388608 | tf_op jit(solution)/shard_map/dot_general | solution.py:141
  452.4 29.7 %all_to_all.27 = bf16[8,512,256]{2,1,0:T(8,128)(2,1)S(1)} all-to-all(bf16[8,512,256]{2,1,0:T(8,128)(2,1)S(1)} %bitcast.150), channel_id=1, replica_groups=mesh['rep'=2,'fs'=32,'tp'=8] {'tp'}, dimensions={0} | all-to-all | bytes 4194304 | tf_op jit(solution)/shard_map/all_to_all | solution.py:57
  482.4 0.8 add_convert_fusion
  (63 shorter events, 5.2 us)
Async XLA Ops:
  0.0 51.1 %copy-start = (f32[8,512]{1,0:T(8,128)S(1)}, f32[8,512]{1,0:T(8,128)}, u32[]{:S(2)}) copy-start(f32[8,512]{1,0:T(8,128)} %param.17) | copy-start | bytes 49156
  2.6 4.5 copy-start.8
  2.6 4.5 copy-start.9
  2.6 4.5 copy-start.4
  2.6 4.5 copy-start.5
  2.6 4.6 copy-start.6
  2.6 4.6 copy-start.7
  2.7 31.6 %all-to-all-start = ((bf16[8,512,256]{1,2,0:T(8,128)(2,1)}), bf16[8,512,256]{1,2,0:T(8,128)(2,1)S(1)}, u32[]{:S(2)}, u32[]{:S(2)}) async-start(bf16[8,512,256]{1,2,0:T(8,128)(2,1)} %broadcast_in_dim.15), calls=%async_computation | async-start | bytes 4194304 | tf_op jit(solution)/shard_map/all_to_all | solution.py:40
  39.3 328.4 %all-to-all-start.1 = ((bf16[32,64,2560]{2,1,0:T(8,128)(2,1)}), bf16[32,64,2560]{2,1,0:T(8,128)(2,1)}, u32[]{:S(2)}, u32[]{:S(2)}) async-start(bf16[32,64,2560]{2,1,0:T(8,128)(2,1)} %stack.2), calls=%async_computation.1 | async-start | bytes 20971520 | tf_op jit(solution)/shard_map/all_to_all | solution.py:21
  50.9 0.7 copy-start.10
  367.7 2.8 copy-start.2
  375.3 1.3 copy-start.1
  413.5 1.0 copy-start.3
  444.5 0.7 copy-start.11
